TPU v7x, 256 devices: a whole 4x4x8 slice. The times are simulated.
256 devices in a mesh: sp: 64 (over z, y, core), tp: 4 (over x).
Axes of the slice: x: 4, y: 4, z: 8, core: 2. Of those that a mesh axis runs over, the one named last changes fastest.
Arguments:
- pooled_in: bfloat16 [65536, 2048], P('sp', 'tp'), may hold values from -6 to 6
- group_map: bfloat16 [4, 512, 512], P('tp'), may hold values from -0.25 to 0.25
- pool_scale: float32 [2048], P('tp'), may hold values from 0.1 to 1.9
- out_weight: bfloat16 [2048, 2048], P('tp'), may hold values from -0.125 to 0.125
- residual: bfloat16 [65536, 2048], P(('sp', 'tp')), may hold values from -6 to 6
- norm_gain: float32 [2048], replicated, may hold values from 0.1 to 1.9
- gate_weight: bfloat16 [64, 2048, 512], P('sp'), may hold values from -0.125 to 0.125
- up_weight: bfloat16 [64, 2048, 512], P('sp'), may hold values from -0.125 to 0.125
- down_weight: bfloat16 [64, 512, 2048], P('sp'), may hold values from -0.25 to 0.25
- route_expert: int32 [65536, 2], P(('sp', 'tp')), may hold values from 0 to 63, all different within a row; in each aligned block of 256 rows (0 to 255, 256 to 511, ...) at most 12 rows name the same one
- route_score: float32 [65536, 2], P(('sp', 'tp')), may hold values from 0.05 to 1
Outputs:
- layer_out: bfloat16 [65536, 2048], P(('sp', 'tp'))
Inputs may be any that keep to these rules, and one draw needn't show every extreme that they name: `route_expert`: each token names 2 different experts. Within each aligned block of 256 tokens (the rows of one device) no expert is named by more than 12 tokens, and in some such block one expert is named by exactly 12.
All inputs are finite; a program needn't handle non-finite values.
Results may differ from a plain program's by a relative error of at most 0.0065.
Values may be sent and summed in bfloat16 or wider, within the bound.
A program may use at most 64 MiB of HBM per device.

v0:
```python
import jax
import jax.numpy as jnp
from jax import lax
from jax.sharding import Mesh
from jax.sharding import PartitionSpec as P

GROUPS = 4
SP = ("sp_0", "sp_1", "sp_2")
SP_TP = ("sp_0", "sp_1", "sp_2", "tp")


def passed_along(shard, axis, by):
    peers = lax.axis_size(axis)
    pairs = [(i, i + by) for i in range(peers) if 0 <= i + by < peers]
    return lax.ppermute(shard, axis, pairs)


def in_blocks(shard, dim, peers):
    before, after = (shard.shape[:dim], shard.shape[dim + 1 :])
    return jnp.moveaxis(shard.reshape(*before, peers, -1, *after), dim, 0)


def in_order(pieces, dim):
    shape = list(pieces.shape[1:])
    shape[dim] *= pieces.shape[0]
    return jnp.moveaxis(pieces, 0, dim).reshape(shape)


def moved_by_axis(pieces, axes, order):
    shape = [lax.axis_size(a) for a in axes]
    pieces = pieces.reshape(*shape, *pieces.shape[1:])
    for k in order:
        pieces = lax.all_to_all(pieces, axes[k], split_axis=k, concat_axis=k, tiled=True)
    return pieces.reshape(-1, *pieces.shape[len(axes) :])


def core_and_chips(shard, groups, order, split_dim, concat_dim):
    peers = lax.axis_size(groups[0]) * lax.axis_size(groups[1])
    pieces = in_blocks(shard, split_dim, peers)
    return in_order(moved_by_axis(pieces, groups, order), concat_dim)


def body(
    pooled_in,
    group_map,
    pool_scale,
    out_weight,
    residual,
    norm_gain,
    gate_weight,
    up_weight,
    down_weight,
    route_expert,
    route_score,
):
    tok_rows = pooled_in.shape[0]
    model_width = residual.shape[1]
    reach = 2**GROUPS - 1
    window = jnp.left_shift(jnp.int32(2), lax.axis_index("tp"))
    earlier = passed_along(pooled_in[tok_rows - reach :], SP, 1)
    extended = jnp.concatenate([earlier, pooled_in], axis=0).astype(jnp.float32)
    running = jnp.zeros((tok_rows, pooled_in.shape[1]), jnp.float32)
    for offset in range(reach + 1):
        running = running + jnp.where(
            offset < window, extended[reach - offset : reach - offset + tok_rows], 0.0
        )
    position = lax.axis_index(SP) * tok_rows + jnp.arange(tok_rows, dtype=jnp.int32)
    counts = jnp.minimum(position + 1, window).astype(jnp.float32)
    contrast = (running / counts[:, None] - pooled_in.astype(jnp.float32)).astype(jnp.bfloat16)
    mixture = jnp.dot(contrast, group_map[0], preferred_element_type=jnp.float32)
    pooled = (mixture * pool_scale[None, :]).astype(jnp.bfloat16)
    row_count = tok_rows // lax.axis_size("tp")
    projected = lax.psum_scatter(
        jnp.dot(pooled, out_weight, preferred_element_type=jnp.float32),
        "tp",
        scatter_dimension=0,
        tiled=True,
    )
    middle = (residual.astype(jnp.float32) + projected).astype(jnp.bfloat16)
    middle_f = middle.astype(jnp.float32)
    factor = lax.rsqrt(jnp.mean(middle_f * middle_f, axis=1, keepdims=True) + 1e-06)
    normed = (middle_f * factor * norm_gain[None, :]).astype(jnp.bfloat16)
    experts = lax.axis_size(SP)
    top_count = route_expert.shape[1]
    capacity = max(2, 3 * row_count * top_count // (2 * experts))
    assign = route_expert.reshape(-1)
    onehot = (assign[:, None] == jnp.arange(experts, dtype=jnp.int32)[None, :]).astype(jnp.int32)
    slot_rank = jnp.sum(jnp.cumsum(onehot, axis=0) * onehot, axis=1) - 1
    slot_index = assign * capacity + slot_rank
    token_of = jnp.arange(assign.shape[0], dtype=jnp.int32) // top_count
    slot_source = jnp.full((experts * capacity,), row_count, jnp.int32).at[slot_index].set(token_of)
    padded_rows = jnp.concatenate([normed, jnp.zeros((1, model_width), jnp.bfloat16)], axis=0)
    outgoing = padded_rows[slot_source].reshape(experts, capacity, model_width)
    received = core_and_chips(outgoing, (("sp_0", "sp_1"), "sp_2"), (0, 1), 0, 0)
    flat_rows = received.reshape(-1, model_width)
    gate_part = jnp.dot(flat_rows, gate_weight[0], preferred_element_type=jnp.float32)
    up_part = jnp.dot(flat_rows, up_weight[0], preferred_element_type=jnp.float32)
    hidden = (jax.nn.silu(gate_part) * up_part).astype(jnp.bfloat16)
    produced = jnp.dot(hidden, down_weight[0], preferred_element_type=jnp.float32).astype(
        jnp.bfloat16
    )
    produced_all = produced.reshape(received.shape)
    returned = lax.all_to_all(produced_all, SP, split_axis=0, concat_axis=0, tiled=True)
    picked = returned.reshape(experts * capacity, model_width)[slot_index].astype(jnp.float32)
    weights = route_score / jnp.sum(route_score, axis=1, keepdims=True)
    combined = jnp.sum(
        picked.reshape(row_count, top_count, model_width) * weights[:, :, None], axis=1
    )
    return (middle_f + combined).astype(jnp.bfloat16)


def solution(mesh):
    split = Mesh(mesh.devices.reshape(8, 4, 2, mesh.shape["tp"]), ("sp_0", "sp_1", "sp_2", "tp"))
    in_specs = (
        P(SP, "tp"),
        P("tp", None, None),
        P("tp"),
        P("tp", None),
        P(SP_TP, None),
        P(),
        P(SP, None, None),
        P(SP, None, None),
        P(SP, None, None),
        P(SP_TP, None),
        P(SP_TP, None),
    )
    out_specs = P(SP_TP, None)
    return jax.shard_map(body, mesh=split, in_specs=in_specs, out_specs=out_specs, check_vma=False)
```

profile of v0, /device:TPU:1, one launch (start us, length us, event | category | flops | bytes accessed | tf_op | source)
XLA Modules:
  0.0 397.4 jit_solution(15256243611029776938)
XLA Ops:
  7.4 4.7 %collective-permute-start = (bf16[15,512]{1,0:T(8,128)(2,1)S(1)}, bf16[15,512]{1,0:T(8,128)(2,1)S(1)}, u32[]{:S(2)}, u32[]{:S(2)}) collective-permute-start(bf16[15,512]{1,0:T(8,128)(2,1)S(1)} %slice.57), channel_id=1, source_target_pairs={{0,4},{4,8},{8,12},{12,16},{16,20},{20,24},{24,28},{28,32},{32,36}... | collective-permute-start | bytes 46088 | tf_op jit(solution)/shard_map/ppermute | solution.py:15
  13.0 2.9 maximum_convert_fusion
  15.9 25.3 %fusion.29 = f32[1024,2048]{1,0:T(8,128)} fusion(bf16[512,2048]{1,0:T(8,128)(2,1)S(1)} %copy-done, f32[512]{0:T(512)S(1)} %copy-done.9, bf16[1024,512]{1,0:T(8,128)(2,1)S(1)} %copy-done.4, f32[1039,512]{1,0:T(8,128)} %maximum_convert_fusion, f32[1024]{0:T(1024)S(1)} %minimum_convert_fusion, pred[]{:T(512)S(6)} %gt.63, pred[]{:T(512)S(6)} %gt.62, ...), kind=kOutput, calls=%fused_computation.54 | convolution fusion | flops 2703753216 | bytes 45619216 | tf_op jit(solution)/shard_map/dot_general | solution.py:74
  44.3 2.4 scatter_custom_fusion
  46.8 81.7 %reduce-scatter.2.cloned.1.call-done = f32[256,2048]{1,0:T(8,128)} async-done(((f32[1024,2048]{1,0:T(8,128)}), f32[256,2048]{1,0:T(8,128)}) %reduce-scatter.2.cloned.1.call-update) | async-done | bytes 2097168 | tf_op jit(solution)/shard_map/reduce_scatter | solution.py:73
  128.6 2.0 fusion
  131.9 4.3 %gather_fusion = bf16[768,2048]{1,0:T(8,128)(2,1)} fusion(bf16[257,2048]{1,0:T(8,128)(2,1)S(1)} %concatenate.7, s32[1024]{0:T(1024)S(1)} %pad_clamp_fusion.1), kind=kCustom, calls=%fused_computation | custom fusion | bytes 6294528 | tf_op jit(solution)/shard_map/gather | solution.py:93
  136.2 6.1 %reshape_reshape_reshape.6 = bf16[32,2,1,12,2048]{4,3,1,0,2:T(8,128)(2,1)} reshape(bf16[768,2048]{1,0:T(8,128)(2,1)} %gather_fusion) | data formatting | bytes 6291456 | tf_op jit(solution)/shard_map/reshape;reshape;reshape | solution.py:31
  142.3 5.5 %copy.22 = bf16[32,2,1,12,2048]{4,1,3,2,0:T(2,128)(2,1)S(1)} copy(bf16[32,2,1,12,2048]{4,3,1,0,2:T(8,128)(2,1)} %reshape_reshape_reshape.6) | data formatting | bytes 6291456 | tf_op jit(solution)/shard_map/reshape;reshape;reshape | solution.py:31
  147.7 80.5 %all_to_all.15 = bf16[32,2,1,12,2048]{4,1,3,2,0:T(2,128)(2,1)S(1)} all-to-all(bf16[32,2,1,12,2048]{4,1,3,2,0:T(2,128)(2,1)S(1)} %copy.22), channel_id=1, replica_groups=mesh['sp_0'=8,'sp_1'=4,'sp_2'=2,'tp'=4] {'sp_0','sp_1'}, dimensions={0} | all-to-all | bytes 6291456 | tf_op jit(solution)/shard_map/all_to_all | solution.py:33
  228.2 1.7 copy.23
  230.0 8.8 %all_to_all.16 = bf16[32,2,1,12,2048]{4,0,3,2,1:T(8,128)(2,1)S(1)} all-to-all(bf16[32,2,1,12,2048]{4,0,3,2,1:T(8,128)(2,1)S(1)} %copy.23), channel_id=1, replica_groups=mesh['sp_0'=8,'sp_1'=4,'sp_2'=2,'tp'=4] {'sp_2'}, dimensions={1} | all-to-all | bytes 6291456 | tf_op jit(solution)/shard_map/all_to_all | solution.py:33
  238.7 3.7 copy.24
  242.4 4.7 %reshape_reshape_reshape.7 = bf16[768,2048]{1,0:T(8,128)(2,1)S(1)} reshape(bf16[32,2,1,12,2048]{4,3,1,0,2:T(8,128)(2,1)} %copy.24) | data formatting | bytes 6291456 | tf_op jit(solution)/shard_map/reshape;reshape;reshape | solution.py:95
  247.2 4.5 %fusion.24 = f32[768,512]{1,0:T(8,128)} fusion(bf16[768,2048]{1,0:T(8,128)(2,1)S(1)} %reshape_reshape_reshape.7, bf16[1,2048,512]{2,1,0:T(8,128)(2,1)} %param.17), kind=kOutput, calls=%fused_computation.48 | convolution fusion | flops 1610612736 | bytes 6815744 | tf_op jit(solution)/shard_map/dot_general | solution.py:96
  251.7 7.9 %convolution_convert_fusion = bf16[768,2048]{1,0:T(8,128)(2,1)} fusion(bf16[1,512,2048]{2,1,0:T(8,128)(2,1)} %param.19, f32[768,512]{1,0:T(8,128)} %fusion.24, bf16[768,2048]{1,0:T(8,128)(2,1)S(1)} %reshape_reshape_reshape.7, bf16[1,2048,512]{2,1,0:T(8,128)(2,1)} %param.18), kind=kOutput, calls=%fused_computation.4 | convolution fusion | flops 3225157632 | bytes 12058624 | tf_op jit(solution)/shard_map/dot_general | solution.py:99
  259.6 6.1 %reshape.81 = bf16[64,12,2048]{2,1,0:T(8,128)(2,1)} reshape(bf16[768,2048]{1,0:T(8,128)(2,1)} %convolution_convert_fusion) | data formatting | bytes 6291456 | tf_op jit(solution)/shard_map/reshape | solution.py:102
  265.6 6.4 %all-to-all-start.2 = ((bf16[64,12,2048]{2,1,0:T(8,128)(2,1)}), bf16[64,12,2048]{2,1,0:T(8,128)(2,1)}, u32[]{:S(2)}, u32[]{:S(2)}) async-start(bf16[64,12,2048]{2,1,0:T(8,128)(2,1)} %reshape.81), calls=%async_computation.3 | async-start | bytes 8388608 | tf_op jit(solution)/shard_map/all_to_all | solution.py:103
  272.3 94.5 %all-to-all-done.2 = bf16[64,12,2048]{2,1,0:T(8,128)(2,1)} async-done(((bf16[64,12,2048]{2,1,0:T(8,128)(2,1)}), bf16[64,12,2048]{2,1,0:T(8,128)(2,1)}, u32[]{:S(2)}, u32[]{:S(2)}) %all-to-all-start.2) | async-done | bytes 3145760 | tf_op jit(solution)/shard_map/all_to_all | solution.py:103
  366.8 4.7 %reshape.82 = bf16[768,2048]{1,0:T(8,128)(2,1)S(1)} reshape(bf16[64,12,2048]{2,1,0:T(8,128)(2,1)} %all-to-all-done.2) | data formatting | bytes 6291456 | tf_op jit(solution)/shard_map/reshape | solution.py:104
  371.5 3.3 gather_fusion.1
  374.8 5.4 %reshape.83 = f32[256,2,2048]{2,1,0:T(2,128)} reshape(bf16[512,2048]{1,0:T(8,128)(2,1)} %gather_fusion.1) | data formatting | bytes 6291456 | tf_op jit(solution)/shard_map/convert_element_type | solution.py:104
  380.3 9.0 %multiply_reduce_fusion = f32[256,2048]{1,0:T(8,128)S(1)} fusion(f32[256,2,2048]{2,1,0:T(2,128)} %reshape.83, f32[256,2]{1,0:T(8,128)S(1)} %copy.25), kind=kLoop, calls=%fused_computation.3 | loop fusion | flops 1572864 | bytes 6293504 | tf_op jit(solution)/shard_map/reduce_sum | solution.py:106
  389.3 1.3 fusion.3
  (49 shorter events, 6.2 us)
Async XLA Ops:
  6.5 9.4 %copy-start = (bf16[512,2048]{1,0:T(8,128)(2,1)S(1)}, bf16[512,2048]{1,0:T(8,128)(2,1)}, u32[]{:S(2)}) copy-start(bf16[512,2048]{1,0:T(8,128)(2,1)} %param.14) | copy-start | bytes 6291460
  6.5 9.4 %copy-start.4 = (bf16[1024,512]{1,0:T(8,128)(2,1)S(1)}, bf16[1024,512]{1,0:T(8,128)(2,1)}, u32[]{:S(2)}) copy-start(bf16[1024,512]{1,0:T(8,128)(2,1)} %param.11) | copy-start | bytes 3145732
  6.5 9.4 %copy-start.9 = (f32[512]{0:T(512)S(1)}, f32[512]{0:T(512)}, u32[]{:S(2)}) copy-start(f32[512]{0:T(512)} %param.13) | copy-start | bytes 6148
  6.5 122.0 %reduce-scatter.2.cloned.1.call-start = ((), (), s32[]{:S(2)}) async-start(), calls=%async_computation.4 | async-start | bytes 10485760 | tf_op jit(solution)/shard_map/reduce_scatter | solution.py:73
  7.4 5.6 %collective-permute-start = (bf16[15,512]{1,0:T(8,128)(2,1)S(1)}, bf16[15,512]{1,0:T(8,128)(2,1)S(1)}, u32[]{:S(2)}, u32[]{:S(2)}) collective-permute-start(bf16[15,512]{1,0:T(8,128)(2,1)S(1)} %slice.57), channel_id=1, source_target_pairs={{0,4},{4,8},{8,12},{12,16},{16,20},{20,24},{24,28},{28,32},{32,36}... | collective-permute-start | bytes 46088 | tf_op jit(solution)/shard_map/ppermute | solution.py:15
  41.3 0.7 copy-start.7
  41.9 86.6 %copy-start.5 = (bf16[256,2048]{1,0:T(8,128)(2,1)S(1)}, bf16[256,2048]{1,0:T(8,128)(2,1)}, u32[]{:S(2)}) copy-start(bf16[256,2048]{1,0:T(8,128)(2,1)} %param.15) | copy-start | bytes 3145732
  46.8 84.7 %copy-start.6 = (f32[2048]{0:T(1024)S(1)}, f32[2048]{0:T(1024)}, u32[]{:S(2)}) copy-start(f32[2048]{0:T(1024)} %param.16) | copy-start | bytes 24580
  130.5 1.0 copy-start.2
  265.6 6.4 %copy-start.8 = (f32[256,2]{0,1:T(2,128)S(1)}, f32[256,2]{0,1:T(2,128)}, u32[]{:S(2)}) copy-start(f32[256,2]{0,1:T(2,128)} %param.21) | copy-start | bytes 6148
  265.6 101.1 %all-to-all-start.2 = ((bf16[64,12,2048]{2,1,0:T(8,128)(2,1)}), bf16[64,12,2048]{2,1,0:T(8,128)(2,1)}, u32[]{:S(2)}, u32[]{:S(2)}) async-start(bf16[64,12,2048]{2,1,0:T(8,128)(2,1)} %reshape.81), calls=%async_computation.3 | async-start | bytes 8388608 | tf_op jit(solution)/shard_map/all_to_all | solution.py:103
  380.2 9.1 %copy-start.3 = (bf16[256,2048]{1,0:T(8,128)(2,1)S(1)}, bf16[256,2048]{1,0:T(8,128)(2,1)}, u32[]{:S(2)}) copy-start(bf16[256,2048]{1,0:T(8,128)(2,1)} %copy-done.2) | copy-start | bytes 3145732
  380.3 10.3 %copy-start.1 = (bf16[512,2048]{1,0:T(8,128)(2,1)S(1)}, bf16[512,2048]{1,0:T(8,128)(2,1)}, u32[]{:S(2)}) copy-start(bf16[512,2048]{1,0:T(8,128)(2,1)} %param.14) | copy-start | bytes 6291460
Sparse Core Ops, SparseCore 0:
  41.4 87.0 reduce-scatter.1
where the time goes:
time: 399 us; the launch traced here: 397 us
  waiting for transfers between devices  177 us (44%)
  blocking collectives  89.3 us (22%)
  local copies, waits for them, and re-layouts  51.6 us (13%)
  matrix products  37.8 us (9%)
  other arithmetic  17 us (4%)
  between operations  13.7 us (3%)
  starting transfers between devices  11.1 us (3%)
    all_to_all x1, waiting for transfers between devices, body(): lax.all_to_all(produced_all, SP, split_axis=0, concat_axis=0, tiled=True)  94.5 us
    all_to_all x2, blocking collectives, moved_by_axis(): lax.all_to_all(pieces, axes[k], split_axis=k, concat_axis=k, tiled=True)  89.3 us
    reduce_scatter x1, waiting for transfers between devices, body(): lax.psum_scatter(jnp.dot(pooled, out_weight, preferred_element_type=jnp.f...  81.7 us
    dot_general x1, matrix products, body(): jnp.dot(pooled, out_weight, preferred_element_type=jnp.float32)  25.3 us
    another operation x2, local copies, waits for them, and re-layouts, moved_by_axis(): pieces = pieces.reshape(*shape, *pieces.shape[1:])  11.5 us
    reduce_sum x1, other arithmetic, body(): jnp.sum(picked.reshape(row_count, top_count, model_width) * weights[:, :,...  9.04 us
  transfers between devices with their start and end apart: 3, of which 3 were waited for; matrix products, arithmetic and copies ran while one was open for 1% of the time, Pallas kernels for 0%

commit v1 on v0

v1 whole, which is shorter than its diff:
```python
import functools

import jax
import jax.numpy as jnp
from jax import lax
from jax.experimental import pallas as pl
from jax.experimental.pallas import tpu as pltpu
from jax.sharding import Mesh
from jax.sharding import PartitionSpec as P

AXES = ("z", "y", "c", "x")
SP = ("z", "y", "c")
MESH = pl.DeviceIdType.MESH
NZ, NY, NC, NX = 8, 4, 2, 4
NSP = NZ * NY * NC
HALO = 16
CAP = 12
BLK = 16
F32, BF16 = jnp.float32, jnp.bfloat16


def dot(a, b):
    return jnp.dot(a, b, preferred_element_type=F32)


def iota(shape, dim):
    return lax.broadcasted_iota(jnp.int32, shape, dim)


def kernel(
    pin_hbm, gm_ref, scale_ref, ow_hbm, res_hbm, gain_ref, wg_hbm, wu_hbm, wd_hbm, re_ref, sc_ref,
    out_ref,
    ext, ow, res, wg, wu, wd, pooled,
    s1, s2, r1, rl, rr, accp, accm, acc, middle, normed,
    mt, mtok, shr, onehot,
    send, recv, ret, back,
    lsem, halo_sem, rs_send, rs_recv, d_send, d_recv, b_send, b_recv,
):
    z, y, c, x = (lax.axis_index(a) for a in AXES)
    me = (z * NY + y) * NC + c
    rows = res_hbm.shape[0]
    width = res_hbm.shape[1]
    tok = pin_hbm.shape[0]
    half = width // 2
    q4 = width // 4

    def sp_peer(idx):
        return (idx // (NY * NC), (idx // NC) % NY, idx % NC, x)

    def x_peer(d):
        return (z, y, c, lax.rem(x + d, NX))

    barrier = pltpu.get_barrier_semaphore()

    def greet(k, carry):
        pl.semaphore_signal(
            barrier, inc=1, device_id=sp_peer(lax.rem(me + k, NSP)), device_id_type=MESH
        )
        return carry

    lax.fori_loop(1, NSP, greet, 0)
    for d in (1, NX - 1):
        pl.semaphore_signal(barrier, inc=1, device_id=x_peer(d), device_id_type=MESH)

    locals_ = [
        pltpu.make_async_copy(src, dst, lsem.at[i])
        for i, (src, dst) in enumerate(
            (
                (pin_hbm, ext.at[pl.ds(HALO, tok), :]),
                (ow_hbm, ow),
                (res_hbm, res),
                (wg_hbm, wg),
                (wu_hbm, wu),
                (wd_hbm, wd),
            )
        )
    ]
    for cp in locals_:
        cp.start()
    pl.semaphore_wait(barrier, NSP - 1 + 2)

    halo = pltpu.make_async_remote_copy(
        src_ref=pin_hbm.at[pl.ds(tok - HALO, HALO), :],
        dst_ref=ext.at[pl.ds(0, HALO), :],
        send_sem=halo_sem.at[0],
        recv_sem=halo_sem.at[1],
        device_id=sp_peer(lax.rem(me + 1, NSP)),
        device_id_type=MESH,
    )
    halo.start()

    lanes = 128
    el = iota((rows, lanes), 1)
    named0 = re_ref[:, 0:1] == el
    named1 = re_ref[:, 1:2] == el
    named = jnp.where(named0 | named1, 1.0, 0.0)
    before = jnp.where(iota((rows, rows), 1) < iota((rows, rows), 0), 1.0, 0.0).astype(BF16)
    rank = dot(before, named.astype(BF16))
    slot = jnp.where(named > 0.5, rank, -1.0)
    mtok[...] = slot.astype(BF16)
    mt[...] = jnp.transpose(slot)
    s0 = sc_ref[:, 0:1]
    s1v = sc_ref[:, 1:2]
    total = s0 + s1v
    shr[...] = (
        jnp.where(named0, s0 / total, 0.0) + jnp.where(named1, s1v / total, 0.0)
    ).astype(BF16)

    window = jnp.left_shift(jnp.int32(2), x)
    step = 128
    lag = iota((step, step + HALO), 0) + HALO - iota((step, step + HALO), 1)
    in_band = jnp.where((lag >= 0) & (lag < window), 1.0, 0.0)
    first_col = iota((step, step + HALO), 1) < HALO

    locals_[0].wait()
    halo.wait()

    def pool(b, carry):
        t0 = pl.multiple_of(b * step, step)
        start_of_all = (me == 0) & (b == 0)
        band = jnp.where(first_col & start_of_all, 0.0, in_band).astype(BF16)
        running = dot(band, ext[pl.ds(t0, step + HALO), :])
        pos = me * tok + t0 + iota((step, 1), 0)
        inverse = 1.0 / jnp.minimum(pos + 1, window).astype(F32)
        own = ext[pl.ds(t0 + HALO, step), :].astype(F32)
        contrast = (running * inverse - own).astype(BF16)
        mixture = dot(contrast, gm_ref[0])
        pooled[pl.ds(t0, step), :] = (mixture * scale_ref[...]).astype(BF16)
        return carry

    lax.fori_loop(0, tok // step, pool, 0)
    locals_[1].wait()

    def partial(d, col):
        base = pl.multiple_of(lax.rem(x + d, NX) * rows, rows)
        return dot(pooled[pl.ds(base, rows), :], ow[:, pl.ds(pl.multiple_of(col, 512), 512)])

    def rs_copy(i, src, dst, d):
        return pltpu.make_async_remote_copy(
            src_ref=src, dst_ref=dst, send_sem=rs_send.at[i], recv_sem=rs_recv.at[i],
            device_id=x_peer(d), device_id_type=MESH,
        )

    lo, hi = pl.ds(0, half), pl.ds(half, half)
    plus1 = rs_copy(0, s1.at[0], r1.at[0], 1)
    minus1 = rs_copy(1, s1.at[1], r1.at[1], NX - 1)
    plus2 = rs_copy(2, s2.at[0, 0], rl.at[1], 1)
    minus2 = rs_copy(3, s2.at[1, 0], rr.at[0], NX - 1)
    plus3 = rs_copy(4, s2.at[0, 1], rl.at[0], 1)
    minus3 = rs_copy(5, s2.at[1, 1], rr.at[1], NX - 1)

    def fill(j, carry):
        col = pl.multiple_of(j * 512, 512)
        s1[0, :, pl.ds(col, 512)] = partial(2, col).astype(BF16)
        s1[1, :, pl.ds(col, 512)] = partial(2, half + col).astype(BF16)
        return carry

    lax.fori_loop(0, half // 512, fill, 0)
    plus1.start()
    minus1.start()

    def fill2(j, carry):
        col = pl.multiple_of(j * 512, 512)
        s2[0, 0, :, pl.ds(col, 512)] = partial(1, half + col).astype(BF16)
        s2[1, 0, :, pl.ds(col, 512)] = partial(NX - 1, col).astype(BF16)
        return carry

    lax.fori_loop(0, half // 512, fill2, 0)
    plus2.start()
    minus2.start()

    def fill3(j, carry):
        col = pl.multiple_of(j * 512, 512)
        accp[:, pl.ds(col, 512)] = partial(1, col)
        accm[:, pl.ds(col, 512)] = partial(NX - 1, half + col)
        return carry

    lax.fori_loop(0, half // 512, fill3, 0)

    def fill4(j, carry):
        col = pl.multiple_of(j * 512, 512)
        acc[:, pl.ds(col, 512)] = partial(0, col)
        return carry

    lax.fori_loop(0, width // 512, fill4, 0)
    plus1.wait_recv()
    s2[0, 1] = (accp[...] + r1[0].astype(F32)).astype(BF16)
    plus3.start()
    minus1.wait_recv()
    s2[1, 1] = (accm[...] + r1[1].astype(F32)).astype(BF16)
    minus3.start()

    lane16 = lax.rem(iota((rows, lanes), 1), BLK)
    tail_at = 3 * (lane16 - CAP)

    def weights_of(g, carry):
        spread = jnp.where(iota((lanes, lanes), 0) == g * 8 + iota((lanes, lanes), 1) // BLK, 1.0, 0.0)
        spread = spread.astype(BF16)
        at = dot(mtok[...], spread)
        share = dot(shr[...], spread)
        for k in range(4):
            if k < 3:
                want = jnp.where(lane16 >= CAP, tail_at + k, -5)
            else:
                want = jnp.where(lane16 < CAP, lane16, -5)
            onehot[k, g] = jnp.where(at == want.astype(F32), share, 0.0).astype(BF16)
        return carry

    lax.fori_loop(0, NZ, weights_of, 0)

    locals_[2].wait()
    plus2.wait_recv()
    minus2.wait_recv()
    plus3.wait_recv()
    minus3.wait_recv()

    def norm(b, carry):
        at = pl.ds(pl.multiple_of(b * 32, 32), 32)
        halves = []
        for h in range(2):
            cols = pl.ds(h * half, half)
            projected = acc[at, cols] + rl[h, at, :].astype(F32) + rr[h, at, :].astype(F32)
            m = (res[at, cols].astype(F32) + projected).astype(BF16)
            middle[at, cols] = m
            halves.append(m.astype(F32))
        squares = sum(jnp.sum(m * m, axis=1, keepdims=True) for m in halves)
        factor = lax.rsqrt(squares / width + 1e-06)
        for h in range(2):
            cols = pl.ds(h * half, half)
            normed[at, cols] = (halves[h] * factor * gain_ref[:, cols]).astype(BF16)
        return carry

    lax.fori_loop(0, rows // 32, norm, 0)

    def dz_of(g):
        return 4 + ((g + 1) // 2) * (1 - 2 * lax.rem(g, 2))

    gl = 8 * BLK
    row16 = lax.rem(iota((gl, rows), 0), BLK)

    def block(idx):
        return pl.ds(pl.multiple_of(idx * BLK, BLK), BLK)

    def peer_index(zz, q):
        return (zz * NY + lax.rem(y + q // NC, NY)) * NC + lax.rem(c + q % NC, NC)

    def out_copy(dest):
        return pltpu.make_async_remote_copy(
            src_ref=send.at[block(dest), :], dst_ref=recv.at[block(me), :],
            send_sem=d_send.at[dest], recv_sem=d_recv.at[me],
            device_id=sp_peer(dest), device_id_type=MESH,
        )

    def out_wait(source):
        return pltpu.make_async_remote_copy(
            src_ref=send.at[block(source), :], dst_ref=recv.at[block(source), :],
            send_sem=d_send.at[source], recv_sem=d_recv.at[source],
            device_id=sp_peer(source), device_id_type=MESH,
        )

    def back_copy(dest):
        return pltpu.make_async_remote_copy(
            src_ref=ret.at[block(dest), :], dst_ref=back.at[block(me), :],
            send_sem=b_send.at[dest], recv_sem=b_recv.at[me],
            device_id=sp_peer(dest), device_id_type=MESH,
        )

    def back_wait(source):
        return pltpu.make_async_remote_copy(
            src_ref=ret.at[block(source), :], dst_ref=back.at[block(source), :],
            send_sem=b_send.at[source], recv_sem=b_recv.at[source],
            device_id=sp_peer(source), device_id_type=MESH,
        )

    def each_peer(g, zz, act):
        for q in range(8):
            idx = peer_index(zz, q)
            if q == 0:
                pl.when(g != NZ - 1)(functools.partial(act, idx))
            else:
                act(idx)

    def dispatch(g, carry):
        zz = lax.rem(z + dz_of(g), NZ)
        at8 = mt[pl.ds(pl.multiple_of(zz * 8, 8), 8), :]
        at = jnp.broadcast_to(at8[:, None, :], (8, BLK, rows)).reshape(gl, rows)
        main = jnp.where(at == jnp.where(row16 < CAP, row16, -5).astype(F32), 1.0, 0.0).astype(BF16)
        at_rows = pl.ds(pl.multiple_of(zz * gl, gl), gl)
        for k in range(3):
            want = jnp.where(row16 >= CAP, 3 * (row16 - CAP) + k, -5).astype(F32)
            tail = jnp.where(at == want, 1.0, 0.0).astype(BF16)
            cols = pl.ds(k * q4, q4)
            packed = dot(main, normed[:, cols]) + dot(tail, normed[:, pl.ds(3 * q4, q4)])
            send[at_rows, cols] = packed.astype(BF16)
        each_peer(g, zz, lambda idx: out_copy(idx).start())

        @pl.when(g == NZ - 1)
        def _():
            recv[block(me), :] = send[block(me), :]

        return carry

    lax.fori_loop(0, NZ, dispatch, 0)
    for i in (3, 4, 5):
        locals_[i].wait()

    ra, ca = iota((gl, gl), 0), iota((gl, gl), 1)
    same = ra // BLK == ca // BLK
    r16, c16 = lax.rem(ra, BLK), lax.rem(ca, BLK)
    keep = lax.rem(iota((gl, q4), 0), BLK) < CAP

    def ffn(g, carry):
        zz = lax.rem(z - dz_of(g) + 2 * NZ, NZ)
        each_peer(g, zz, lambda idx: out_wait(idx).wait_recv())
        at_rows = pl.ds(pl.multiple_of(zz * gl, gl), gl)
        tail = jnp.zeros((gl, q4), F32)
        for k in range(3):
            pick = jnp.where(same & (c16 >= CAP) & (r16 == 3 * (c16 - CAP) + k), 1.0, 0.0)
            tail = tail + dot(pick.astype(BF16), recv[at_rows, pl.ds(k * q4, q4)])
        tail = tail.astype(BF16)
        rows_in = recv[at_rows, :]
        gate = dot(rows_in, wg[pl.ds(0, 3 * q4), :]) + dot(tail, wg[pl.ds(3 * q4, q4), :])
        up = dot(rows_in, wu[pl.ds(0, 3 * q4), :]) + dot(tail, wu[pl.ds(3 * q4, q4), :])
        hidden = (gate / (1.0 + jnp.exp(-gate)) * up).astype(BF16)
        last = dot(hidden, wd[:, pl.ds(3 * q4, q4)]).astype(BF16)
        for k in range(3):
            put = jnp.where(same & (r16 >= CAP) & (c16 == 3 * (r16 - CAP) + k), 1.0, 0.0)
            cols = pl.ds(k * q4, q4)
            ret[at_rows, cols] = jnp.where(
                keep, dot(hidden, wd[:, cols]), dot(put.astype(BF16), last)
            ).astype(BF16)
        each_peer(g, zz, lambda idx: back_copy(idx).start())

        @pl.when(g == NZ - 1)
        def _():
            back[block(me), :] = ret[block(me), :]

        return carry

    lax.fori_loop(0, NZ, ffn, 0)

    def clear(b, carry):
        at = pl.ds(pl.multiple_of(b * 32, 32), 32)
        acc[at, :] = middle[at, :].astype(F32)
        return carry

    lax.fori_loop(0, rows // 32, clear, 0)

    def combine(g, carry):
        zz = lax.rem(z + dz_of(g), NZ)
        each_peer(g, zz, lambda idx: back_wait(idx).wait_recv())
        at_rows = pl.ds(pl.multiple_of(zz * gl, gl), gl)
        extra = acc[:, pl.ds(3 * q4, q4)]
        for k in range(3):
            cols = pl.ds(k * q4, q4)
            piece = back[at_rows, cols]
            acc[:, cols] += dot(onehot[3, zz], piece)
            extra = extra + dot(onehot[k, zz], piece)
        acc[:, pl.ds(3 * q4, q4)] = extra
        return carry

    lax.fori_loop(0, NZ, combine, 0)

    def finish(b, carry):
        at = pl.ds(pl.multiple_of(b * 32, 32), 32)
        out_ref[at, :] = acc[at, :].astype(BF16)
        return carry

    lax.fori_loop(0, rows // 32, finish, 0)
    for cp in (plus1, minus1, plus2, minus2, plus3, minus3):
        cp.wait_send()

    def drain(k, carry):
        idx = lax.rem(me + k, NSP)
        out_copy(idx).wait_send()
        back_copy(idx).wait_send()
        return carry

    lax.fori_loop(1, NSP, drain, 0)


def body(
    pooled_in, group_map, pool_scale, out_weight, residual, norm_gain,
    gate_weight, up_weight, down_weight, route_expert, route_score,
):
    tok, ch = pooled_in.shape
    rows, width = residual.shape
    ff = gate_weight.shape[2]
    half = width // 2
    packed = (NSP * BLK, 3 * width // 4)
    vmem = pl.BlockSpec(memory_space=pltpu.VMEM)
    hbm = pl.BlockSpec(memory_space=pl.ANY)
    dma = pltpu.SemaphoreType.DMA
    return pl.pallas_call(
        kernel,
        out_shape=jax.ShapeDtypeStruct((rows, width), BF16),
        in_specs=[hbm, vmem, vmem, hbm, hbm, vmem, hbm, hbm, hbm, vmem, vmem],
        out_specs=vmem,
        scratch_shapes=[
            pltpu.VMEM((HALO + tok, ch), BF16),
            pltpu.VMEM((ch, width), BF16),
            pltpu.VMEM((rows, width), BF16),
            pltpu.VMEM((width, ff), BF16),
            pltpu.VMEM((width, ff), BF16),
            pltpu.VMEM((ff, width), BF16),
            pltpu.VMEM((tok, ch), BF16),
            pltpu.VMEM((2, rows, half), BF16),
            pltpu.VMEM((2, 2, rows, half), BF16),
            pltpu.VMEM((2, rows, half), BF16),
            pltpu.VMEM((2, rows, half), BF16),
            pltpu.VMEM((2, rows, half), BF16),
            pltpu.VMEM((rows, half), F32),
            pltpu.VMEM((rows, half), F32),
            pltpu.VMEM((rows, width), F32),
            pltpu.VMEM((rows, width), BF16),
            pltpu.VMEM((rows, width), BF16),
            pltpu.VMEM((128, rows), F32),
            pltpu.VMEM((rows, 128), BF16),
            pltpu.VMEM((rows, 128), BF16),
            pltpu.VMEM((4, NZ, rows, 128), BF16),
            pltpu.VMEM(packed, BF16),
            pltpu.VMEM(packed, BF16),
            pltpu.VMEM(packed, BF16),
            pltpu.VMEM(packed, BF16),
            dma((6,)),
            dma((2,)),
            dma((6,)),
            dma((6,)),
            dma((NSP,)),
            dma((NSP,)),
            dma((NSP,)),
            dma((NSP,)),
        ],
        compiler_params=pltpu.CompilerParams(
            collective_id=0, has_side_effects=True, vmem_limit_bytes=60 * 2**20
        ),
    )(
        pooled_in, group_map, pool_scale.reshape(1, -1), out_weight, residual,
        norm_gain.reshape(1, -1), gate_weight.reshape(width, ff), up_weight.reshape(width, ff),
        down_weight.reshape(ff, width), route_expert, route_score,
    )


def solution(mesh):
    split = Mesh(mesh.devices.reshape(NZ, NY, NC, NX), AXES)
    sp_tp = AXES
    in_specs = (
        P(SP, "x"),
        P("x", None, None),
        P("x"),
        P("x", None),
        P(sp_tp, None),
        P(),
        P(SP, None, None),
        P(SP, None, None),
        P(SP, None, None),
        P(sp_tp, None),
        P(sp_tp, None),
    )
    return jax.shard_map(
        body, mesh=split, in_specs=in_specs, out_specs=P(sp_tp, None), check_vma=False
    )
```

time: 399 us -> 207 us (0.52)
  Pallas kernels: 0 us -> 202 us
  waiting for transfers between devices: 177 us -> 0 us
  blocking collectives: 89.3 us -> 0 us
  local copies, waits for them, and re-layouts: 51.6 us -> 5.24 us
  matrix products: 37.8 us -> 0 us
  other arithmetic: 17 us -> 0 us
  between operations: 13.7 us -> 0.01 us
  starting transfers between devices: 11.1 us -> 0 us
    pallas_call x0 -> x1, Pallas kernels: none -> 202 us  [body(): pl.pallas_call(kernel, out_shape=jax.ShapeDtypeStruct((rows, width), BF16...]
    all_to_all x1 -> x0, waiting for transfers between devices: 94.5 us -> none  [body(): lax.all_to_all(produced_all, SP, split_axis=0, concat_axis=0, tiled=True)]
    all_to_all x2 -> x0, blocking collectives: 89.3 us -> none  [moved_by_axis(): lax.all_to_all(pieces, axes[k], split_axis=k, concat_axis=k, tiled=True)]
    reduce_scatter x1 -> x0, waiting for transfers between devices: 81.7 us -> none  [body(): lax.psum_scatter(jnp.dot(pooled, out_weight, preferred_element_type=jnp.f...]
    dot_general x3 -> x0, matrix products: 37.8 us -> none  [the longest x1 25.3 us: body(): jnp.dot(pooled, out_weight, preferred_element_type=jnp.float32)]
    another operation x4 -> x0, local copies, waits for them, and re-layouts: 16.3 us -> none  [the longest x2 11.5 us: moved_by_axis(): pieces = pieces.reshape(*shape, *pieces.shape[1:])]
    reduce_sum x4 -> x0, other arithmetic: 11.2 us -> none  [the longest x1 9.04 us: body(): jnp.sum(picked.reshape(row_count, top_count, model_width) * weights[:, :,...]
    reshape x2 -> x0, local copies, waits for them, and re-layouts: 10.8 us -> none  [the longest x1 6.07 us: body(): produced_all = produced.reshape(received.shape)]
  transfers between devices with their start and end apart: 3 -> 0, of which waited for: 3 -> 0; matrix products, arithmetic and copies ran while one was open for 1% -> 0% of each run, Pallas kernels for 0% -> 0%
where the time goes in v1:
time: 207 us
  Pallas kernels  202 us (98%)
  local copies, waits for them, and re-layouts  5.24 us (3%)
    pallas_call x1, Pallas kernels, body(): pl.pallas_call(kernel, out_shape=jax.ShapeDtypeStruct((rows, width), BF16...  202 us
    unnamed x3, local copies, waits for them, and re-layouts  5.24 us

profile of v1, /device:TPU:1, one launch (start us, length us, event | category | flops | bytes accessed | tf_op | source)
XLA Modules:
  0.0 207.2 jit_solution(791016080862792502)
XLA Ops:
  0.0 1.5 copy.12.re_ref
  1.5 1.5 copy.13.sc_ref
  2.9 201.9 %shard_map.109 = bf16[256,2048]{1,0:T(8,128)(2,1)} custom-call(bf16[1024,512]{1,0:T(8,128)(2,1)} %pin_hbm.1, bf16[1,512,512]{2,1,0:T(8,128)(2,1)} %gm_ref.1, f32[1,512]{1,0:T(1,128)} %bitcast.9, bf16[512,2048]{1,0:T(8,128)(2,1)} %ow_hbm.1, bf16[256,2048]{1,0:T(8,128)(2,1)} %res_hbm.1, f32[1,2048]{1,0:T(1,128)} %bitcast.8, bf16[2048,512]{1,0:T(8,128)(2,1)} %bitcast.5, ...), custom_call_target="tpu_custom_call" | custom-call | tf_op jit(solution)/shard_map/pallas_call | solution.py:394
  204.9 2.3 %copy.15 = bf16[256,2048]{1,0:T(8,128)(2,1)} copy(bf16[256,2048]{1,0:T(8,128)(2,1)} %shard_map.109) | data formatting | bytes 2097152

commit v2 on v1

--- a/solution.py
+++ b/solution.py
@@ -30,11 +30,11 @@
 def kernel(
     pin_hbm, gm_ref, scale_ref, ow_hbm, res_hbm, gain_ref, wg_hbm, wu_hbm, wd_hbm, re_ref, sc_ref,
     out_ref,
-    ext, ow, res, wg, wu, wd, pooled,
+    ext, ow, res, wg, wu, wd, wg2, wu2, wd2, pooled,
     s1, s2, r1, rl, rr, accp, accm, acc, middle, normed,
     mt, mtok, shr, onehot,
     send, recv, ret, back,
-    lsem, halo_sem, rs_send, rs_recv, d_send, d_recv, b_send, b_recv,
+    lsem, halo_sem, w_send, w_recv, rs_send, rs_recv, d_send, d_recv, b_send, b_recv,
 ):
     z, y, c, x = (lax.axis_index(a) for a in AXES)
     me = (z * NY + y) * NC + c
@@ -44,8 +44,10 @@
     half = width // 2
     q4 = width // 4
 
-    def sp_peer(idx):
-        return (idx // (NY * NC), (idx // NC) % NY, idx % NC, x)
+    def sp_peer(idx, xx=x):
+        return (idx // (NY * NC), (idx // NC) % NY, idx % NC, xx)
+
+    mirror = NX - 1 - x
 
     def x_peer(d):
         return (z, y, c, lax.rem(x + d, NX))
@@ -53,14 +55,19 @@
     barrier = pltpu.get_barrier_semaphore()
 
     def greet(k, carry):
+        other = lax.rem(k, 2)
         pl.semaphore_signal(
-            barrier, inc=1, device_id=sp_peer(lax.rem(me + k, NSP)), device_id_type=MESH
-        )
-        return carry
-
-    lax.fori_loop(1, NSP, greet, 0)
-    for d in (1, NX - 1):
-        pl.semaphore_signal(barrier, inc=1, device_id=x_peer(d), device_id_type=MESH)
+            barrier,
+            inc=1,
+            device_id=sp_peer(lax.rem(me + k // 2, NSP), x + other * (mirror - x)),
+            device_id_type=MESH,
+        )
+        return carry
+
+    lax.fori_loop(1, 2 * NSP, greet, 0)
+    pl.semaphore_signal(
+        barrier, inc=1, device_id=(z, y, c, x + 1 - 2 * lax.rem(x, 2)), device_id_type=MESH
+    )
 
     locals_ = [
         pltpu.make_async_copy(src, dst, lsem.at[i])
@@ -77,7 +84,23 @@
     ]
     for cp in locals_:
         cp.start()
-    pl.semaphore_wait(barrier, NSP - 1 + 2)
+    pl.semaphore_wait(barrier, 2 * NSP)
+
+    gives = c == x // 2
+
+    def weight_copy(i, side):
+        src = (wg_hbm, wu_hbm, wd_hbm)[i]
+        dst = (wg2, wu2, wd2)[i]
+        return pltpu.make_async_remote_copy(
+            src_ref=src, dst_ref=dst, send_sem=w_send.at[2 * i + side], recv_sem=w_recv.at[i],
+            device_id=(lax.rem(z + (1, NZ - 1)[side], NZ), y, side, x), device_id_type=MESH,
+        )
+
+    @pl.when(gives)
+    def _():
+        for i in range(3):
+            for side in range(2):
+                weight_copy(i, side).start()
 
     halo = pltpu.make_async_remote_copy(
         src_ref=pin_hbm.at[pl.ds(tok - HALO, HALO), :],
@@ -232,112 +255,145 @@
 
     lax.fori_loop(0, rows // 32, norm, 0)
 
-    def dz_of(g):
+    def lag_of(g):
         return 4 + ((g + 1) // 2) * (1 - 2 * lax.rem(g, 2))
 
     gl = 8 * BLK
     row16 = lax.rem(iota((gl, rows), 0), BLK)
+    sign = 1 - 2 * c
 
     def block(idx):
         return pl.ds(pl.multiple_of(idx * BLK, BLK), BLK)
 
-    def peer_index(zz, q):
-        return (zz * NY + lax.rem(y + q // NC, NY)) * NC + lax.rem(c + q % NC, NC)
-
-    def out_copy(dest):
+    def place(lag, yy, cc):
+        ze = lax.rem(z - lag + NZ, NZ)
+        own = lag == 0
+        plus = (lag < 4) | ((lag == 4) & (c == 0))
+        shift = jnp.where(own, 0, jnp.where(plus, 1, NZ - 1))
+        j = jnp.where(plus, lag - 1, 7 - lag)
+        away = jnp.where(x // 2 == cc, 0, 1)
+        core = jnp.where(own, cc, jnp.where(plus, 0, 1))
+        xx = jnp.where(own | (away == 0), x, mirror)
+        slot = jnp.where(
+            own, y * 2 + c, jnp.where(j < 3, 8 + 16 * j + (y * 2 + c) * 2 + away, 56 + y * 2 + away)
+        )
+        dev = (lax.rem(ze + shift, NZ), yy, core, xx)
+        return (ze * NY + yy) * NC + cc, dev, slot
+
+    def is_me(dev):
+        return (dev[0] == z) & (dev[1] == y) & (dev[2] == c) & (dev[3] == x)
+
+    def origin(slot_group, yy, cc, away):
+        if slot_group == "own":
+            return (z, yy, cc, x), yy * 2 + cc, me
+        j = slot_group
+        zz = lax.rem(z + sign * j + NZ, NZ)
+        xx = jnp.where(away == 0, x, mirror)
+        slot = jnp.where(j < 3, 8 + 16 * j + (yy * 2 + cc) * 2 + away, 56 + yy * 2 + away)
+        return (zz, yy, cc, xx), slot, imported
+
+    imported = (lax.rem(z - sign + NZ, NZ) * NY + y) * NC + x // 2
+
+    def members(group, act):
+        if isinstance(group, str):
+            todo = [(q // NC, q % NC, 0) for q in range(8)]
+        elif isinstance(group, int):
+            todo = [(q, c, away) for q in range(4) for away in range(2)]
+        else:
+            todo = [(q // NC, q % NC, away) for q in range(8) for away in range(2)]
+        for q, cc, away in todo:
+            core = cc if isinstance(group, int) else lax.rem(c + cc, NC)
+            dev, slot, expert = origin(group, lax.rem(y + q, NY), core, away)
+            pl.when(jnp.logical_not(is_me(dev)))(functools.partial(act, dev, slot, expert))
+
+    def out_copy(expert, dev, slot):
         return pltpu.make_async_remote_copy(
-            src_ref=send.at[block(dest), :], dst_ref=recv.at[block(me), :],
-            send_sem=d_send.at[dest], recv_sem=d_recv.at[me],
-            device_id=sp_peer(dest), device_id_type=MESH,
-        )
-
-    def out_wait(source):
+            src_ref=send.at[block(expert), :], dst_ref=recv.at[block(slot), :],
+            send_sem=d_send.at[expert], recv_sem=d_recv.at[slot],
+            device_id=dev, device_id_type=MESH,
+        )
+
+    def back_copy(dev, slot, expert):
         return pltpu.make_async_remote_copy(
-            src_ref=send.at[block(source), :], dst_ref=recv.at[block(source), :],
-            send_sem=d_send.at[source], recv_sem=d_recv.at[source],
-            device_id=sp_peer(source), device_id_type=MESH,
-        )
-
-    def back_copy(dest):
+            src_ref=ret.at[block(slot), :], dst_ref=back.at[block(expert), :],
+            send_sem=b_send.at[slot], recv_sem=b_recv.at[expert],
+            device_id=dev, device_id_type=MESH,
+        )
+
+    def back_wait(expert, dev):
         return pltpu.make_async_remote_copy(
-            src_ref=ret.at[block(dest), :], dst_ref=back.at[block(me), :],
-            send_sem=b_send.at[dest], recv_sem=b_recv.at[me],
-            device_id=sp_peer(dest), device_id_type=MESH,
-        )
-
-    def back_wait(source):
-        return pltpu.make_async_remote_copy(
-            src_ref=ret.at[block(source), :], dst_ref=back.at[block(source), :],
-            send_sem=b_send.at[source], recv_sem=b_recv.at[source],
-            device_id=sp_peer(source), device_id_type=MESH,
-        )
-
-    def each_peer(g, zz, act):
+            src_ref=ret.at[block(expert), :], dst_ref=back.at[block(expert), :],
+            send_sem=b_send.at[expert], recv_sem=b_recv.at[expert],
+            device_id=dev, device_id_type=MESH,
+        )
+
+    def each_expert(lag, act):
         for q in range(8):
-            idx = peer_index(zz, q)
-            if q == 0:
-                pl.when(g != NZ - 1)(functools.partial(act, idx))
-            else:
-                act(idx)
+            expert, dev, slot = place(lag, lax.rem(y + q // NC, NY), lax.rem(c + q % NC, NC))
+            pl.when(jnp.logical_not(is_me(dev)))(functools.partial(act, expert, dev, slot))
 
     def dispatch(g, carry):
-        zz = lax.rem(z + dz_of(g), NZ)
-        at8 = mt[pl.ds(pl.multiple_of(zz * 8, 8), 8), :]
+        lag = lag_of(g)
+        ze = lax.rem(z - lag + NZ, NZ)
+        at8 = mt[pl.ds(pl.multiple_of(ze * 8, 8), 8), :]
         at = jnp.broadcast_to(at8[:, None, :], (8, BLK, rows)).reshape(gl, rows)
         main = jnp.where(at == jnp.where(row16 < CAP, row16, -5).astype(F32), 1.0, 0.0).astype(BF16)
-        at_rows = pl.ds(pl.multiple_of(zz * gl, gl), gl)
+        at_rows = pl.ds(pl.multiple_of(ze * gl, gl), gl)
         for k in range(3):
             want = jnp.where(row16 >= CAP, 3 * (row16 - CAP) + k, -5).astype(F32)
             tail = jnp.where(at == want, 1.0, 0.0).astype(BF16)
             cols = pl.ds(k * q4, q4)
             packed = dot(main, normed[:, cols]) + dot(tail, normed[:, pl.ds(3 * q4, q4)])
             send[at_rows, cols] = packed.astype(BF16)
-        each_peer(g, zz, lambda idx: out_copy(idx).start())
-
-        @pl.when(g == NZ - 1)
-        def _():
-            recv[block(me), :] = send[block(me), :]
-
+        each_expert(lag, lambda expert, dev, slot: out_copy(expert, dev, slot).start())
         return carry
 
     lax.fori_loop(0, NZ, dispatch, 0)
+    own_slot, far_slot = y * 2 + c, 8 + (y * 2 + c) * 2
+    recv[block(own_slot), :] = send[block(me), :]
+    recv[block(far_slot), :] = send[block(imported), :]
     for i in (3, 4, 5):
         locals_[i].wait()
 
-    ra, ca = iota((gl, gl), 0), iota((gl, gl), 1)
-    same = ra // BLK == ca // BLK
-    r16, c16 = lax.rem(ra, BLK), lax.rem(ca, BLK)
-    keep = lax.rem(iota((gl, q4), 0), BLK) < CAP
-
-    def ffn(g, carry):
-        zz = lax.rem(z - dz_of(g) + 2 * NZ, NZ)
-        each_peer(g, zz, lambda idx: out_wait(idx).wait_recv())
-        at_rows = pl.ds(pl.multiple_of(zz * gl, gl), gl)
-        tail = jnp.zeros((gl, q4), F32)
+    def ffn(group, first, count, gate_w, up_w, down_w):
+        members(group, lambda dev, slot, expert: out_copy(slot, dev, slot).wait_recv())
+        ra, ca = iota((count, count), 0), iota((count, count), 1)
+        same = ra // BLK == ca // BLK
+        r16, c16 = lax.rem(ra, BLK), lax.rem(ca, BLK)
+        keep = lax.rem(iota((count, q4), 0), BLK) < CAP
+        at_rows = pl.ds(pl.multiple_of(first * BLK, 128), count)
+        tail = jnp.zeros((count, q4), F32)
         for k in range(3):
             pick = jnp.where(same & (c16 >= CAP) & (r16 == 3 * (c16 - CAP) + k), 1.0, 0.0)
             tail = tail + dot(pick.astype(BF16), recv[at_rows, pl.ds(k * q4, q4)])
         tail = tail.astype(BF16)
         rows_in = recv[at_rows, :]
-        gate = dot(rows_in, wg[pl.ds(0, 3 * q4), :]) + dot(tail, wg[pl.ds(3 * q4, q4), :])
-        up = dot(rows_in, wu[pl.ds(0, 3 * q4), :]) + dot(tail, wu[pl.ds(3 * q4, q4), :])
+        gate = dot(rows_in, gate_w[pl.ds(0, 3 * q4), :]) + dot(tail, gate_w[pl.ds(3 * q4, q4), :])
+        up = dot(rows_in, up_w[pl.ds(0, 3 * q4), :]) + dot(tail, up_w[pl.ds(3 * q4, q4), :])
         hidden = (gate / (1.0 + jnp.exp(-gate)) * up).astype(BF16)
-        last = dot(hidden, wd[:, pl.ds(3 * q4, q4)]).astype(BF16)
+        last = dot(hidden, down_w[:, pl.ds(3 * q4, q4)]).astype(BF16)
         for k in range(3):
             put = jnp.where(same & (r16 >= CAP) & (c16 == 3 * (r16 - CAP) + k), 1.0, 0.0)
             cols = pl.ds(k * q4, q4)
             ret[at_rows, cols] = jnp.where(
-                keep, dot(hidden, wd[:, cols]), dot(put.astype(BF16), last)
+                keep, dot(hidden, down_w[:, cols]), dot(put.astype(BF16), last)
             ).astype(BF16)
-        each_peer(g, zz, lambda idx: back_copy(idx).start())
-
-        @pl.when(g == NZ - 1)
-        def _():
-            back[block(me), :] = ret[block(me), :]
-
-        return carry
-
-    lax.fori_loop(0, NZ, ffn, 0)
+        members(group, lambda dev, slot, expert: back_copy(dev, slot, expert).start())
+
+    ffn("own", 0, 8 * BLK, wg, wu, wd)
+    back[block(me), :] = ret[block(own_slot), :]
+    for i in range(3):
+        weight_copy(i, 0).wait_recv()
+
+    def far(i, carry):
+        j = jnp.where(i == 0, 0, 3 - i)
+        ffn(j, 8 + 16 * j, 16 * BLK, wg2, wu2, wd2)
+        return carry
+
+    lax.fori_loop(0, 1, far, 0)
+    back[block(imported), :] = ret[block(far_slot), :]
+    ffn(3, 56, 8 * BLK, wg2, wu2, wd2)
+    lax.fori_loop(1, 3, far, 0)
 
     def clear(b, carry):
         at = pl.ds(pl.multiple_of(b * 32, 32), 32)
@@ -347,8 +403,10 @@
     lax.fori_loop(0, rows // 32, clear, 0)
 
     def combine(g, carry):
-        zz = lax.rem(z + dz_of(g), NZ)
-        each_peer(g, zz, lambda idx: back_wait(idx).wait_recv())
+        lag = jnp.where(g < 2, g, jnp.where(g == 2, 7, jnp.where(g == 3, 4, jnp.where(
+            g < 6, 2 * g - 5, 4 * g - 22))))
+        zz = lax.rem(z - lag + NZ, NZ)
+        each_expert(lag, lambda expert, dev, slot: back_wait(expert, dev).wait_recv())
         at_rows = pl.ds(pl.multiple_of(zz * gl, gl), gl)
         extra = acc[:, pl.ds(3 * q4, q4)]
         for k in range(3):
@@ -370,13 +428,25 @@
     for cp in (plus1, minus1, plus2, minus2, plus3, minus3):
         cp.wait_send()
 
-    def drain(k, carry):
-        idx = lax.rem(me + k, NSP)
-        out_copy(idx).wait_send()
-        back_copy(idx).wait_send()
-        return carry
-
-    lax.fori_loop(1, NSP, drain, 0)
+    def drain(g, carry):
+        each_expert(g, lambda expert, dev, slot: out_copy(expert, dev, slot).wait_send())
+        return carry
+
+    lax.fori_loop(0, NZ, drain, 0)
+    members("own", lambda dev, slot, expert: back_copy(dev, slot, expert).wait_send())
+    members(3, lambda dev, slot, expert: back_copy(dev, slot, expert).wait_send())
+
+    def drain_far(j, carry):
+        members(j, lambda dev, slot, expert: back_copy(dev, slot, expert).wait_send())
+        return carry
+
+    lax.fori_loop(0, 3, drain_far, 0)
+
+    @pl.when(gives)
+    def _():
+        for i in range(3):
+            for side in range(2):
+                weight_copy(i, side).wait_send()
 
 
 def body(
@@ -400,6 +470,9 @@
             pltpu.VMEM((HALO + tok, ch), BF16),
             pltpu.VMEM((ch, width), BF16),
             pltpu.VMEM((rows, width), BF16),
+            pltpu.VMEM((width, ff), BF16),
+            pltpu.VMEM((width, ff), BF16),
+            pltpu.VMEM((ff, width), BF16),
             pltpu.VMEM((width, ff), BF16),
             pltpu.VMEM((width, ff), BF16),
             pltpu.VMEM((ff, width), BF16),
@@ -425,6 +498,8 @@
             dma((6,)),
             dma((2,)),
             dma((6,)),
+            dma((3,)),
+            dma((6,)),
             dma((6,)),
             dma((NSP,)),
             dma((NSP,)),

time: 207 us -> 212 us (1.024)
  Pallas kernels: 202 us -> 206 us
    pallas_call x1, Pallas kernels: 202 us -> 206 us  [body(): pl.pallas_call(kernel, out_shape=jax.ShapeDtypeStruct((rows, width), BF16...]
where the time goes in v2:
time: 212 us; the launch traced here: 211 us
  Pallas kernels  206 us (97%)
  local copies, waits for them, and re-layouts  5.24 us (2%)
    pallas_call x1, Pallas kernels, body(): pl.pallas_call(kernel, out_shape=jax.ShapeDtypeStruct((rows, width), BF16...  206 us
    unnamed x3, local copies, waits for them, and re-layouts  5.24 us

profile of v2, /device:TPU:1, one launch (start us, length us, event | category | flops | bytes accessed | tf_op | source)
XLA Modules:
  0.0 211.5 jit_solution(7830878360974066072)
XLA Ops:
  0.0 1.5 copy.12.re_ref
  1.5 1.5 copy.13.sc_ref
  2.9 206.2 %shard_map.109 = bf16[256,2048]{1,0:T(8,128)(2,1)} custom-call(bf16[1024,512]{1,0:T(8,128)(2,1)} %pin_hbm.1, bf16[1,512,512]{2,1,0:T(8,128)(2,1)} %gm_ref.1, f32[1,512]{1,0:T(1,128)} %bitcast.9, bf16[512,2048]{1,0:T(8,128)(2,1)} %ow_hbm.1, bf16[256,2048]{1,0:T(8,128)(2,1)} %res_hbm.1, f32[1,2048]{1,0:T(1,128)} %bitcast.8, bf16[2048,512]{1,0:T(8,128)(2,1)} %bitcast.5, ...), custom_call_target="tpu_custom_call" | custom-call | tf_op jit(solution)/shard_map/pallas_call | solution.py:464
  209.2 2.3 %copy.15 = bf16[256,2048]{1,0:T(8,128)(2,1)} copy(bf16[256,2048]{1,0:T(8,128)(2,1)} %shard_map.109) | data formatting | bytes 2097152

commit v3 on v2

--- a/solution.py
+++ b/solution.py
@@ -34,7 +34,7 @@
     s1, s2, r1, rl, rr, accp, accm, acc, middle, normed,
     mt, mtok, shr, onehot,
     send, recv, ret, back,
-    lsem, halo_sem, w_send, w_recv, rs_send, rs_recv, d_send, d_recv, b_send, b_recv,
+    lsem, gate_sem, halo_sem, w_send, w_recv, rs_send, rs_recv, d_send, d_recv, b_send, b_recv,
 ):
     z, y, c, x = (lax.axis_index(a) for a in AXES)
     me = (z * NY + y) * NC + c
@@ -54,20 +54,18 @@
 
     barrier = pltpu.get_barrier_semaphore()
 
-    def greet(k, carry):
-        other = lax.rem(k, 2)
-        pl.semaphore_signal(
-            barrier,
-            inc=1,
-            device_id=sp_peer(lax.rem(me + k // 2, NSP), x + other * (mirror - x)),
-            device_id_type=MESH,
-        )
-        return carry
-
-    lax.fori_loop(1, 2 * NSP, greet, 0)
-    pl.semaphore_signal(
-        barrier, inc=1, device_id=(z, y, c, x + 1 - 2 * lax.rem(x, 2)), device_id_type=MESH
-    )
+    lines = [(z, y, 1 - c, x), (z, y, c, mirror), (z, y, c, x + 1 - 2 * lax.rem(x, 2))]
+    y_line = [(z, lax.rem(y + k, NY), c, x) for k in range(1, NY)]
+    lines += y_line + [(lax.rem(z + k, NZ), y, c, x) for k in range(1, NZ)]
+    lines.append(sp_peer(lax.rem(me + 2 * c - 1 + NSP, NSP)))
+    lines += [(lax.rem(z + k, NZ), y, 1 - c, x) for k in (1, NZ - 1)]
+    for dev in lines:
+        pl.semaphore_signal(barrier, inc=1, device_id=dev, device_id_type=MESH)
+
+    def stage(i, devs):
+        for dev in devs:
+            pl.semaphore_signal(gate_sem.at[i], inc=1, device_id=dev, device_id_type=MESH)
+        pl.semaphore_wait(gate_sem.at[i], len(devs))
 
     locals_ = [
         pltpu.make_async_copy(src, dst, lsem.at[i])
@@ -84,23 +82,7 @@
     ]
     for cp in locals_:
         cp.start()
-    pl.semaphore_wait(barrier, 2 * NSP)
-
-    gives = c == x // 2
-
-    def weight_copy(i, side):
-        src = (wg_hbm, wu_hbm, wd_hbm)[i]
-        dst = (wg2, wu2, wd2)[i]
-        return pltpu.make_async_remote_copy(
-            src_ref=src, dst_ref=dst, send_sem=w_send.at[2 * i + side], recv_sem=w_recv.at[i],
-            device_id=(lax.rem(z + (1, NZ - 1)[side], NZ), y, side, x), device_id_type=MESH,
-        )
-
-    @pl.when(gives)
-    def _():
-        for i in range(3):
-            for side in range(2):
-                weight_copy(i, side).start()
+    pl.semaphore_wait(barrier, len(lines))
 
     halo = pltpu.make_async_remote_copy(
         src_ref=pin_hbm.at[pl.ds(tok - HALO, HALO), :],
@@ -112,18 +94,39 @@
     )
     halo.start()
 
+    gives = c == x // 2
+
+    def weight_copy(i, side):
+        src = (wg_hbm, wu_hbm, wd_hbm)[i]
+        dst = (wg2, wu2, wd2)[i]
+        return pltpu.make_async_remote_copy(
+            src_ref=src, dst_ref=dst, send_sem=w_send.at[2 * i + side], recv_sem=w_recv.at[i],
+            device_id=(lax.rem(z + (1, NZ - 1)[side], NZ), y, side, x), device_id_type=MESH,
+        )
+
+    @pl.when(gives)
+    def _():
+        for i in range(3):
+            for side in range(2):
+                weight_copy(i, side).start()
+
     lanes = 128
     el = iota((rows, lanes), 1)
-    named0 = re_ref[:, 0:1] == el
-    named1 = re_ref[:, 1:2] == el
+    mt[...] = jnp.zeros((lanes, rows), F32)
+    mt[0:2, :] = re_ref[...].astype(F32)
+    mt[2:4, :] = sc_ref[...]
+    by_token = jnp.transpose(mt[...])
+    el_f = el.astype(F32)
+    named0 = by_token[:, 0:1] == el_f
+    named1 = by_token[:, 1:2] == el_f
     named = jnp.where(named0 | named1, 1.0, 0.0)
     before = jnp.where(iota((rows, rows), 1) < iota((rows, rows), 0), 1.0, 0.0).astype(BF16)
     rank = dot(before, named.astype(BF16))
     slot = jnp.where(named > 0.5, rank, -1.0)
     mtok[...] = slot.astype(BF16)
     mt[...] = jnp.transpose(slot)
-    s0 = sc_ref[:, 0:1]
-    s1v = sc_ref[:, 1:2]
+    s0 = by_token[:, 2:3]
+    s1v = by_token[:, 3:4]
     total = s0 + s1v
     shr[...] = (
         jnp.where(named0, s0 / total, 0.0) + jnp.where(named1, s1v / total, 0.0)
@@ -135,6 +138,7 @@
     in_band = jnp.where((lag >= 0) & (lag < window), 1.0, 0.0)
     first_col = iota((step, step + HALO), 1) < HALO
 
+    stage(0, y_line)
     locals_[0].wait()
     halo.wait()
 
@@ -152,6 +156,7 @@
         return carry
 
     lax.fori_loop(0, tok // step, pool, 0)
+    stage(1, lines[:1])
     locals_[1].wait()
 
     def partial(d, col):
@@ -181,6 +186,7 @@
     lax.fori_loop(0, half // 512, fill, 0)
     plus1.start()
     minus1.start()
+    stage(2, lines[1:2])
 
     def fill2(j, carry):
         col = pl.multiple_of(j * 512, 512)
@@ -496,6 +502,7 @@
             pltpu.VMEM(packed, BF16),
             pltpu.VMEM(packed, BF16),
             dma((6,)),
+            pltpu.SemaphoreType.REGULAR((3,)),
             dma((2,)),
             dma((6,)),
             dma((3,)),
@@ -512,7 +519,7 @@
     )(
         pooled_in, group_map, pool_scale.reshape(1, -1), out_weight, residual,
         norm_gain.reshape(1, -1), gate_weight.reshape(width, ff), up_weight.reshape(width, ff),
-        down_weight.reshape(ff, width), route_expert, route_score,
+        down_weight.reshape(ff, width), route_expert.T, route_score.T,
     )
 
 

time: 212 us -> 168 us (0.79)
  Pallas kernels: 206 us -> 166 us
  local copies, waits for them, and re-layouts: 5.24 us -> 2.3 us
    pallas_call x1, Pallas kernels: 206 us -> 166 us  [body(): pl.pallas_call(kernel, out_shape=jax.ShapeDtypeStruct((rows, width), BF16...]
    unnamed x3 -> x1, local copies, waits for them, and re-layouts: 5.24 us -> 2.3 us
where the time goes in v3:
time: 168 us
  Pallas kernels  166 us (99%)
  local copies, waits for them, and re-layouts  2.3 us (1%)
    pallas_call x1, Pallas kernels, body(): pl.pallas_call(kernel, out_shape=jax.ShapeDtypeStruct((rows, width), BF16...  166 us

profile of v3, /device:TPU:1, one launch (start us, length us, event | category | flops | bytes accessed | tf_op | source)
XLA Modules:
  0.0 168.1 jit_solution(5521168991971963121)
XLA Ops:
  0.0 165.8 %shard_map.109 = bf16[256,2048]{1,0:T(8,128)(2,1)} custom-call(bf16[1024,512]{1,0:T(8,128)(2,1)} %pin_hbm.1, bf16[1,512,512]{2,1,0:T(8,128)(2,1)} %gm_ref.1, f32[1,512]{1,0:T(1,128)} %bitcast.11, bf16[512,2048]{1,0:T(8,128)(2,1)} %ow_hbm.1, bf16[256,2048]{1,0:T(8,128)(2,1)} %res_hbm.1, f32[1,2048]{1,0:T(1,128)} %bitcast.10, bf16[2048,512]{1,0:T(8,128)(2,1)} %bitcast.7, ...), custom_call_target="tpu_custom_call" | custom-call | tf_op jit(solution)/shard_map/pallas_call | solution.py:470
  165.8 2.3 %copy.13 = bf16[256,2048]{1,0:T(8,128)(2,1)} copy(bf16[256,2048]{1,0:T(8,128)(2,1)} %shard_map.109) | data formatting | bytes 2097152

commit v4 on v3

--- a/solution.py
+++ b/solution.py
@@ -34,7 +34,7 @@
     s1, s2, r1, rl, rr, accp, accm, acc, middle, normed,
     mt, mtok, shr, onehot,
     send, recv, ret, back,
-    lsem, gate_sem, halo_sem, w_send, w_recv, rs_send, rs_recv, d_send, d_recv, b_send, b_recv,
+    lsem, gate_sem, halo_sem, swap_sem, w_send, w_recv, rs_send, rs_recv, d_send, d_recv, b_send, b_recv,
 ):
     z, y, c, x = (lax.axis_index(a) for a in AXES)
     me = (z * NY + y) * NC + c
@@ -96,13 +96,24 @@
 
     gives = c == x // 2
 
+    mid = wd_hbm.shape[0] // 2
+    pair = x + 1 - 2 * lax.rem(x, 2)
+
+    def my_half(ref):
+        return ref.at[pl.ds(pl.multiple_of(lax.rem(x, 2) * mid, mid), mid), :]
+
     def weight_copy(i, side):
-        src = (wg_hbm, wu_hbm, wd_hbm)[i]
-        dst = (wg2, wu2, wd2)[i]
+        src = (my_half(wd_hbm), wg_hbm, wu_hbm)[i]
+        dst = (my_half(wd2), wg2, wu2)[i]
         return pltpu.make_async_remote_copy(
             src_ref=src, dst_ref=dst, send_sem=w_send.at[2 * i + side], recv_sem=w_recv.at[i],
             device_id=(lax.rem(z + (1, NZ - 1)[side], NZ), y, side, x), device_id_type=MESH,
         )
+
+    swap = pltpu.make_async_remote_copy(
+        src_ref=my_half(wd2), dst_ref=my_half(wd2), send_sem=swap_sem.at[0], recv_sem=swap_sem.at[1],
+        device_id=(z, y, c, pair), device_id_type=MESH,
+    )
 
     @pl.when(gives)
     def _():
@@ -140,9 +151,14 @@
 
     stage(0, y_line)
     locals_[0].wait()
-    halo.wait()
-
-    def pool(b, carry):
+    halo.wait_recv()
+
+    per = rows // step
+
+    def pool(i, carry):
+        part = i // per
+        d = jnp.where(part == 0, 2, jnp.where(part == 3, 0, 2 * part - 1))
+        b = lax.rem(x + d, NX) * per + lax.rem(i, per)
         t0 = pl.multiple_of(b * step, step)
         start_of_all = (me == 0) & (b == 0)
         band = jnp.where(first_col & start_of_all, 0.0, in_band).astype(BF16)
@@ -155,7 +171,7 @@
         pooled[pl.ds(t0, step), :] = (mixture * scale_ref[...]).astype(BF16)
         return carry
 
-    lax.fori_loop(0, tok // step, pool, 0)
+    lax.fori_loop(0, per, pool, 0)
     stage(1, lines[:1])
     locals_[1].wait()
 
@@ -187,6 +203,7 @@
     plus1.start()
     minus1.start()
     stage(2, lines[1:2])
+    lax.fori_loop(per, NX * per, pool, 0)
 
     def fill2(j, carry):
         col = pl.multiple_of(j * 512, 512)
@@ -218,6 +235,8 @@
     minus1.wait_recv()
     s2[1, 1] = (accm[...] + r1[1].astype(F32)).astype(BF16)
     minus3.start()
+    weight_copy(0, 0).wait_recv()
+    swap.start()
 
     lane16 = lax.rem(iota((rows, lanes), 1), BLK)
     tail_at = 3 * (lane16 - CAP)
@@ -388,8 +407,9 @@
 
     ffn("own", 0, 8 * BLK, wg, wu, wd)
     back[block(me), :] = ret[block(own_slot), :]
-    for i in range(3):
+    for i in (1, 2):
         weight_copy(i, 0).wait_recv()
+    swap.wait_recv()
 
     def far(i, carry):
         j = jnp.where(i == 0, 0, 3 - i)
@@ -447,6 +467,9 @@
         return carry
 
     lax.fori_loop(0, 3, drain_far, 0)
+
+    halo.wait_send()
+    swap.wait_send()
 
     @pl.when(gives)
     def _():
@@ -504,6 +527,7 @@
             dma((6,)),
             pltpu.SemaphoreType.REGULAR((3,)),
             dma((2,)),
+            dma((2,)),
             dma((6,)),
             dma((3,)),
             dma((6,)),

time: 168 us -> 157 us (0.935)
  Pallas kernels: 166 us -> 155 us
    pallas_call x1, Pallas kernels: 166 us -> 155 us  [body(): pl.pallas_call(kernel, out_shape=jax.ShapeDtypeStruct((rows, width), BF16...]
where the time goes in v4:
time: 157 us
  Pallas kernels  155 us (99%)
  local copies, waits for them, and re-layouts  2.3 us (1%)
    pallas_call x1, Pallas kernels, body(): pl.pallas_call(kernel, out_shape=jax.ShapeDtypeStruct((rows, width), BF16...  155 us

profile of v4, /device:TPU:1, one launch (start us, length us, event | category | flops | bytes accessed | tf_op | source)
XLA Modules:
  0.0 157.0 jit_solution(16989661939853813184)
XLA Ops:
  0.0 154.7 %shard_map.109 = bf16[256,2048]{1,0:T(8,128)(2,1)} custom-call(bf16[1024,512]{1,0:T(8,128)(2,1)} %pin_hbm.1, bf16[1,512,512]{2,1,0:T(8,128)(2,1)} %gm_ref.1, f32[1,512]{1,0:T(1,128)} %bitcast.11, bf16[512,2048]{1,0:T(8,128)(2,1)} %ow_hbm.1, bf16[256,2048]{1,0:T(8,128)(2,1)} %res_hbm.1, f32[1,2048]{1,0:T(1,128)} %bitcast.10, bf16[2048,512]{1,0:T(8,128)(2,1)} %bitcast.7, ...), custom_call_target="tpu_custom_call" | custom-call | tf_op jit(solution)/shard_map/pallas_call | solution.py:493
  154.7 2.3 %copy.13 = bf16[256,2048]{1,0:T(8,128)(2,1)} copy(bf16[256,2048]{1,0:T(8,128)(2,1)} %shard_map.109) | data formatting | bytes 2097152

commit v5 on v4

--- a/solution.py
+++ b/solution.py
@@ -120,6 +120,93 @@
         for i in range(3):
             for side in range(2):
                 weight_copy(i, side).start()
+
+    window = jnp.left_shift(jnp.int32(2), x)
+    step = 128
+    lag = iota((step, step + HALO), 0) + HALO - iota((step, step + HALO), 1)
+    in_band = jnp.where((lag >= 0) & (lag < window), 1.0, 0.0)
+    first_col = iota((step, step + HALO), 1) < HALO
+
+    locals_[0].wait()
+    pl.when(x == 2)(halo.wait_recv)
+
+    per = rows // step
+
+    def pool(i, carry):
+        part = i // per
+        d = jnp.where(part == 0, 2, jnp.where(part == 3, 0, 2 * part - 1))
+        b = lax.rem(x + d, NX) * per + lax.rem(i, per)
+        t0 = pl.multiple_of(b * step, step)
+        start_of_all = (me == 0) & (b == 0)
+        band = jnp.where(first_col & start_of_all, 0.0, in_band).astype(BF16)
+        running = dot(band, ext[pl.ds(t0, step + HALO), :])
+        pos = me * tok + t0 + iota((step, 1), 0)
+        inverse = 1.0 / jnp.minimum(pos + 1, window).astype(F32)
+        own = ext[pl.ds(t0 + HALO, step), :].astype(F32)
+        contrast = (running * inverse - own).astype(BF16)
+        mixture = dot(contrast, gm_ref[0])
+        pooled[pl.ds(t0, step), :] = (mixture * scale_ref[...]).astype(BF16)
+        return carry
+
+    lax.fori_loop(0, per, pool, 0)
+    locals_[1].wait()
+
+    def partial(d, col):
+        base = pl.multiple_of(lax.rem(x + d, NX) * rows, rows)
+        return dot(pooled[pl.ds(base, rows), :], ow[:, pl.ds(pl.multiple_of(col, 512), 512)])
+
+    def rs_copy(i, src, dst, d):
+        return pltpu.make_async_remote_copy(
+            src_ref=src, dst_ref=dst, send_sem=rs_send.at[i], recv_sem=rs_recv.at[i],
+            device_id=x_peer(d), device_id_type=MESH,
+        )
+
+    lo, hi = pl.ds(0, half), pl.ds(half, half)
+    plus1 = rs_copy(0, s1.at[0], r1.at[0], 1)
+    minus1 = rs_copy(1, s1.at[1], r1.at[1], NX - 1)
+    plus2 = rs_copy(2, s2.at[0, 0], rl.at[1], 1)
+    minus2 = rs_copy(3, s2.at[1, 0], rr.at[0], NX - 1)
+    plus3 = rs_copy(4, s2.at[0, 1], rl.at[0], 1)
+    minus3 = rs_copy(5, s2.at[1, 1], rr.at[1], NX - 1)
+
+    def fill(j, carry):
+        col = pl.multiple_of(j * 512, 512)
+        s1[0, :, pl.ds(col, 512)] = partial(2, col).astype(BF16)
+        s1[1, :, pl.ds(col, 512)] = partial(2, half + col).astype(BF16)
+        return carry
+
+    lax.fori_loop(0, half // 512, fill, 0)
+    plus1.start()
+    minus1.start()
+    pl.when(x != 2)(halo.wait_recv)
+    lax.fori_loop(per, NX * per, pool, 0)
+
+    def fill2(j, carry):
+        col = pl.multiple_of(j * 512, 512)
+        s2[0, 0, :, pl.ds(col, 512)] = partial(1, half + col).astype(BF16)
+        s2[1, 0, :, pl.ds(col, 512)] = partial(NX - 1, col).astype(BF16)
+        return carry
+
+    lax.fori_loop(0, half // 512, fill2, 0)
+    plus2.start()
+    minus2.start()
+    stage(0, y_line)
+
+    def fill3(j, carry):
+        col = pl.multiple_of(j * 512, 512)
+        accp[:, pl.ds(col, 512)] = partial(1, col)
+        accm[:, pl.ds(col, 512)] = partial(NX - 1, half + col)
+        return carry
+
+    lax.fori_loop(0, half // 512, fill3, 0)
+
+    def fill4(j, carry):
+        col = pl.multiple_of(j * 512, 512)
+        acc[:, pl.ds(col, 512)] = partial(0, col)
+        return carry
+
+    lax.fori_loop(0, width // 512, fill4, 0)
+    stage(1, lines[:1])
 
     lanes = 128
     el = iota((rows, lanes), 1)
@@ -143,92 +230,6 @@
         jnp.where(named0, s0 / total, 0.0) + jnp.where(named1, s1v / total, 0.0)
     ).astype(BF16)
 
-    window = jnp.left_shift(jnp.int32(2), x)
-    step = 128
-    lag = iota((step, step + HALO), 0) + HALO - iota((step, step + HALO), 1)
-    in_band = jnp.where((lag >= 0) & (lag < window), 1.0, 0.0)
-    first_col = iota((step, step + HALO), 1) < HALO
-
-    stage(0, y_line)
-    locals_[0].wait()
-    halo.wait_recv()
-
-    per = rows // step
-
-    def pool(i, carry):
-        part = i // per
-        d = jnp.where(part == 0, 2, jnp.where(part == 3, 0, 2 * part - 1))
-        b = lax.rem(x + d, NX) * per + lax.rem(i, per)
-        t0 = pl.multiple_of(b * step, step)
-        start_of_all = (me == 0) & (b == 0)
-        band = jnp.where(first_col & start_of_all, 0.0, in_band).astype(BF16)
-        running = dot(band, ext[pl.ds(t0, step + HALO), :])
-        pos = me * tok + t0 + iota((step, 1), 0)
-        inverse = 1.0 / jnp.minimum(pos + 1, window).astype(F32)
-        own = ext[pl.ds(t0 + HALO, step), :].astype(F32)
-        contrast = (running * inverse - own).astype(BF16)
-        mixture = dot(contrast, gm_ref[0])
-        pooled[pl.ds(t0, step), :] = (mixture * scale_ref[...]).astype(BF16)
-        return carry
-
-    lax.fori_loop(0, per, pool, 0)
-    stage(1, lines[:1])
-    locals_[1].wait()
-
-    def partial(d, col):
-        base = pl.multiple_of(lax.rem(x + d, NX) * rows, rows)
-        return dot(pooled[pl.ds(base, rows), :], ow[:, pl.ds(pl.multiple_of(col, 512), 512)])
-
-    def rs_copy(i, src, dst, d):
-        return pltpu.make_async_remote_copy(
-            src_ref=src, dst_ref=dst, send_sem=rs_send.at[i], recv_sem=rs_recv.at[i],
-            device_id=x_peer(d), device_id_type=MESH,
-        )
-
-    lo, hi = pl.ds(0, half), pl.ds(half, half)
-    plus1 = rs_copy(0, s1.at[0], r1.at[0], 1)
-    minus1 = rs_copy(1, s1.at[1], r1.at[1], NX - 1)
-    plus2 = rs_copy(2, s2.at[0, 0], rl.at[1], 1)
-    minus2 = rs_copy(3, s2.at[1, 0], rr.at[0], NX - 1)
-    plus3 = rs_copy(4, s2.at[0, 1], rl.at[0], 1)
-    minus3 = rs_copy(5, s2.at[1, 1], rr.at[1], NX - 1)
-
-    def fill(j, carry):
-        col = pl.multiple_of(j * 512, 512)
-        s1[0, :, pl.ds(col, 512)] = partial(2, col).astype(BF16)
-        s1[1, :, pl.ds(col, 512)] = partial(2, half + col).astype(BF16)
-        return carry
-
-    lax.fori_loop(0, half // 512, fill, 0)
-    plus1.start()
-    minus1.start()
-    stage(2, lines[1:2])
-    lax.fori_loop(per, NX * per, pool, 0)
-
-    def fill2(j, carry):
-        col = pl.multiple_of(j * 512, 512)
-        s2[0, 0, :, pl.ds(col, 512)] = partial(1, half + col).astype(BF16)
-        s2[1, 0, :, pl.ds(col, 512)] = partial(NX - 1, col).astype(BF16)
-        return carry
-
-    lax.fori_loop(0, half // 512, fill2, 0)
-    plus2.start()
-    minus2.start()
-
-    def fill3(j, carry):
-        col = pl.multiple_of(j * 512, 512)
-        accp[:, pl.ds(col, 512)] = partial(1, col)
-        accm[:, pl.ds(col, 512)] = partial(NX - 1, half + col)
-        return carry
-
-    lax.fori_loop(0, half // 512, fill3, 0)
-
-    def fill4(j, carry):
-        col = pl.multiple_of(j * 512, 512)
-        acc[:, pl.ds(col, 512)] = partial(0, col)
-        return carry
-
-    lax.fori_loop(0, width // 512, fill4, 0)
     plus1.wait_recv()
     s2[0, 1] = (accp[...] + r1[0].astype(F32)).astype(BF16)
     plus3.start()
@@ -237,6 +238,7 @@
     minus3.start()
     weight_copy(0, 0).wait_recv()
     swap.start()
+    stage(2, lines[1:2])
 
     lane16 = lax.rem(iota((rows, lanes), 1), BLK)
     tail_at = 3 * (lane16 - CAP)

time: 157 us -> 157 us (level)
  no operation moved by 1% of the time
where the time goes in v5:
time: 157 us
  Pallas kernels  155 us (99%)
  local copies, waits for them, and re-layouts  2.3 us (1%)
    pallas_call x1, Pallas kernels, body(): pl.pallas_call(kernel, out_shape=jax.ShapeDtypeStruct((rows, width), BF16...  155 us

profile of v5, /device:TPU:1, one launch (start us, length us, event | category | flops | bytes accessed | tf_op | source)
XLA Modules:
  0.0 156.9 jit_solution(4944981192079955098)
XLA Ops:
  0.0 154.6 %shard_map.109 = bf16[256,2048]{1,0:T(8,128)(2,1)} custom-call(bf16[1024,512]{1,0:T(8,128)(2,1)} %pin_hbm.1, bf16[1,512,512]{2,1,0:T(8,128)(2,1)} %gm_ref.1, f32[1,512]{1,0:T(1,128)} %bitcast.11, bf16[512,2048]{1,0:T(8,128)(2,1)} %ow_hbm.1, bf16[256,2048]{1,0:T(8,128)(2,1)} %res_hbm.1, f32[1,2048]{1,0:T(1,128)} %bitcast.10, bf16[2048,512]{1,0:T(8,128)(2,1)} %bitcast.7, ...), custom_call_target="tpu_custom_call" | custom-call | tf_op jit(solution)/shard_map/pallas_call | solution.py:495
  154.6 2.3 %copy.13 = bf16[256,2048]{1,0:T(8,128)(2,1)} copy(bf16[256,2048]{1,0:T(8,128)(2,1)} %shard_map.109) | data formatting | bytes 2097152

commit v6 on v5

--- a/solution.py
+++ b/solution.py
@@ -99,25 +99,31 @@
     mid = wd_hbm.shape[0] // 2
     pair = x + 1 - 2 * lax.rem(x, 2)
 
-    def my_half(ref):
-        return ref.at[pl.ds(pl.multiple_of(lax.rem(x, 2) * mid, mid), mid), :]
+    share = 3 * wu_hbm.shape[0] // 8
+    rest = pl.ds(2 * share, wu_hbm.shape[0] - 2 * share)
+
+    def mine(ref, count):
+        return ref.at[pl.ds(pl.multiple_of(lax.rem(x, 2) * count, count), count), :]
 
     def weight_copy(i, side):
-        src = (my_half(wd_hbm), wg_hbm, wu_hbm)[i]
-        dst = (my_half(wd2), wg2, wu2)[i]
+        src = (mine(wd_hbm, mid), mine(wu_hbm, share), wg_hbm, wu_hbm.at[rest, :])[i]
+        dst = (mine(wd2, mid), mine(wu2, share), wg2, wu2.at[rest, :])[i]
         return pltpu.make_async_remote_copy(
             src_ref=src, dst_ref=dst, send_sem=w_send.at[2 * i + side], recv_sem=w_recv.at[i],
             device_id=(lax.rem(z + (1, NZ - 1)[side], NZ), y, side, x), device_id_type=MESH,
         )
 
-    swap = pltpu.make_async_remote_copy(
-        src_ref=my_half(wd2), dst_ref=my_half(wd2), send_sem=swap_sem.at[0], recv_sem=swap_sem.at[1],
-        device_id=(z, y, c, pair), device_id_type=MESH,
-    )
+    swaps = [
+        pltpu.make_async_remote_copy(
+            src_ref=part, dst_ref=part, send_sem=swap_sem.at[2 * i], recv_sem=swap_sem.at[2 * i + 1],
+            device_id=(z, y, c, pair), device_id_type=MESH,
+        )
+        for i, part in enumerate((mine(wd2, mid), mine(wu2, share)))
+    ]
 
     @pl.when(gives)
     def _():
-        for i in range(3):
+        for i in range(4):
             for side in range(2):
                 weight_copy(i, side).start()
 
@@ -236,8 +242,9 @@
     minus1.wait_recv()
     s2[1, 1] = (accm[...] + r1[1].astype(F32)).astype(BF16)
     minus3.start()
-    weight_copy(0, 0).wait_recv()
-    swap.start()
+    for i, swap in enumerate(swaps):
+        weight_copy(i, 0).wait_recv()
+        swap.start()
     stage(2, lines[1:2])
 
     lane16 = lax.rem(iota((rows, lanes), 1), BLK)
@@ -409,9 +416,10 @@
 
     ffn("own", 0, 8 * BLK, wg, wu, wd)
     back[block(me), :] = ret[block(own_slot), :]
-    for i in (1, 2):
+    for i in (2, 3):
         weight_copy(i, 0).wait_recv()
-    swap.wait_recv()
+    for swap in swaps:
+        swap.wait_recv()
 
     def far(i, carry):
         j = jnp.where(i == 0, 0, 3 - i)
@@ -471,11 +479,12 @@
     lax.fori_loop(0, 3, drain_far, 0)
 
     halo.wait_send()
-    swap.wait_send()
+    for swap in swaps:
+        swap.wait_send()
 
     @pl.when(gives)
     def _():
-        for i in range(3):
+        for i in range(4):
             for side in range(2):
                 weight_copy(i, side).wait_send()
 
@@ -529,9 +538,9 @@
             dma((6,)),
             pltpu.SemaphoreType.REGULAR((3,)),
             dma((2,)),
-            dma((2,)),
-            dma((6,)),
-            dma((3,)),
+            dma((4,)),
+            dma((8,)),
+            dma((4,)),
             dma((6,)),
             dma((6,)),
             dma((NSP,)),

time: 157 us -> 149 us (0.949)
  Pallas kernels: 155 us -> 147 us
    pallas_call x1, Pallas kernels: 155 us -> 147 us  [body(): pl.pallas_call(kernel, out_shape=jax.ShapeDtypeStruct((rows, width), BF16...]
where the time goes in v6:
time: 149 us
  Pallas kernels  147 us (99%)
  local copies, waits for them, and re-layouts  2.3 us (2%)
    pallas_call x1, Pallas kernels, body(): pl.pallas_call(kernel, out_shape=jax.ShapeDtypeStruct((rows, width), BF16...  147 us

profile of v6, /device:TPU:1, one launch (start us, length us, event | category | flops | bytes accessed | tf_op | source)
XLA Modules:
  0.0 148.9 jit_solution(10363341244467387945)
XLA Ops:
  0.0 146.5 %shard_map.109 = bf16[256,2048]{1,0:T(8,128)(2,1)} custom-call(bf16[1024,512]{1,0:T(8,128)(2,1)} %pin_hbm.1, bf16[1,512,512]{2,1,0:T(8,128)(2,1)} %gm_ref.1, f32[1,512]{1,0:T(1,128)} %bitcast.11, bf16[512,2048]{1,0:T(8,128)(2,1)} %ow_hbm.1, bf16[256,2048]{1,0:T(8,128)(2,1)} %res_hbm.1, f32[1,2048]{1,0:T(1,128)} %bitcast.10, bf16[2048,512]{1,0:T(8,128)(2,1)} %bitcast.7, ...), custom_call_target="tpu_custom_call" | custom-call | tf_op jit(solution)/shard_map/pallas_call | solution.py:504
  146.5 2.3 %copy.13 = bf16[256,2048]{1,0:T(8,128)(2,1)} copy(bf16[256,2048]{1,0:T(8,128)(2,1)} %shard_map.109) | data formatting | bytes 2097152

commit v7 on v6

--- a/solution.py
+++ b/solution.py
@@ -99,7 +99,7 @@
     mid = wd_hbm.shape[0] // 2
     pair = x + 1 - 2 * lax.rem(x, 2)
 
-    share = 3 * wu_hbm.shape[0] // 8
+    share = 7 * wu_hbm.shape[0] // 16
     rest = pl.ds(2 * share, wu_hbm.shape[0] - 2 * share)
 
     def mine(ref, count):

time: 149 us -> 148 us (level)
  no operation moved by 1% of the time
where the time goes in v7:
time: 148 us
  Pallas kernels  146 us (99%)
  local copies, waits for them, and re-layouts  2.3 us (2%)
    pallas_call x1, Pallas kernels, body(): pl.pallas_call(kernel, out_shape=jax.ShapeDtypeStruct((rows, width), BF16...  146 us

profile of v7, /device:TPU:1, one launch (start us, length us, event | category | flops | bytes accessed | tf_op | source)
XLA Modules:
  0.0 147.9 jit_solution(5699164345284466916)
XLA Ops:
  0.0 145.5 %shard_map.109 = bf16[256,2048]{1,0:T(8,128)(2,1)} custom-call(bf16[1024,512]{1,0:T(8,128)(2,1)} %pin_hbm.1, bf16[1,512,512]{2,1,0:T(8,128)(2,1)} %gm_ref.1, f32[1,512]{1,0:T(1,128)} %bitcast.11, bf16[512,2048]{1,0:T(8,128)(2,1)} %ow_hbm.1, bf16[256,2048]{1,0:T(8,128)(2,1)} %res_hbm.1, f32[1,2048]{1,0:T(1,128)} %bitcast.10, bf16[2048,512]{1,0:T(8,128)(2,1)} %bitcast.7, ...), custom_call_target="tpu_custom_call" | custom-call | tf_op jit(solution)/shard_map/pallas_call | solution.py:504
  145.5 2.3 %copy.13 = bf16[256,2048]{1,0:T(8,128)(2,1)} copy(bf16[256,2048]{1,0:T(8,128)(2,1)} %shard_map.109) | data formatting | bytes 2097152
